TPU v7x, 512 devices: a 4x2x32 block of a 4x8x32 slice. The times are simulated.
512 devices in a mesh: grp: 2 (over y), kv: 64 (over z, core), tp: 4 (over x).
Axes of the slice: x: 4, y: 2, z: 32, core: 2. Of those that a mesh axis runs over, the one named last changes fastest.
The devices are a block of a 4x8x32 slice.
Arguments:
- piece_rows: bfloat16 [8192, 2048], P(('grp', 'kv')), parts along dimension 0, may hold values from -6 to 6
- dec_rows: bfloat16 [256, 2048], P(('grp', 'kv')), parts along dimension 0, may hold values from -6 to 6
- norm_gain: float32 [2048], replicated, may hold values from 0.1 to 1.9
- w_query: bfloat16 [2048, 1024], P(None, 'tp'), may hold values from -0.25 to 0.25
- w_key: bfloat16 [2048, 256], P(None, 'tp'), may hold values from -0.125 to 0.125
- w_value: bfloat16 [2048, 256], P(None, 'tp'), may hold values from -0.125 to 0.125
- w_forget: bfloat16 [2048, 16], P(None, 'tp'), may hold values from -0.125 to 0.125
- forget_bias: float32 [16], P('tp'), may hold values from 3 to 12
- piece_decay: float32 [16, 8192], P('tp', ('grp', 'kv')), parts along dimension 1, may hold values from -3 to 0
- cache_kv: bfloat16 [98304, 4, 128], P(('grp', 'kv'), 'tp'), parts along dimension 0, may hold values from -150 to 150
- cache_gate: float32 [16, 98304], P('tp', ('grp', 'kv')), parts along dimension 1, may hold values from -2460.6 to 0, as said below
- dec_cache: bfloat16 [256, 3072, 4, 128], P(('grp', 'kv'), None, 'tp'), parts along dimension 0, may hold values from -150 to 150
- dec_gate: float32 [256, 16, 3072], P(('grp', 'kv'), 'tp'), parts along dimension 0, may hold values from -156.6 to 0, as said below
- dec_lengths: int32 [256], P(('grp', 'kv')), parts along dimension 0, may hold values from 1 to 3072, as said below
- w_out: bfloat16 [1024, 2048], P(None, 'tp'), may hold values from -0.75 to 0.75
Outputs:
- piece_out: bfloat16 [8192, 2048], P(('grp', 'kv'), 'tp'), parts along dimension 0
- dec_out: bfloat16 [256, 2048], P(('grp', 'kv'), 'tp'), parts along dimension 0
There are 2 independent parts, one for each index of `grp`. A program takes and returns all parts, laid end to end along the dimension named above; an argument that names none is the same for every part. Nothing has to cross between parts.
Inputs may be any that keep to these rules, and one draw needn't show every extreme that they name: `cache_gate`: each head's values never fall from one position to the next and are 0 at the last cached position. `dec_gate`: each sequence's and head's values never rise from one position to the next. Sequence b's cache holds its first dec_lengths[b] positions; in each part some sequence holds 3072.
All inputs are finite; a program needn't handle non-finite values.
Results may differ from a plain program's by a relative error of at most 0.006.
The roundings to bfloat16 on the way count: a program that leaves them out, or rounds other values in their place, can miss the bound.
Values may be sent and summed in bfloat16 or wider, within the bound.
No kernel may reach another device: no remote copies, remote signals or barrier semaphores. Data moves between devices by JAX's collectives and lax.ppermute only.
A program may use at most 64 MiB of HBM per device.

v0:
```python
import jax
import jax.numpy as jnp
from jax import lax
from jax.sharding import Mesh
from jax.sharding import PartitionSpec as P

KV = ("kv_0", "kv_1")
GRP_KV = ("grp", "kv_0", "kv_1")


def carried_in(array, axis, combine, identity):
    length, mine = (lax.axis_size(axis), lax.axis_index(axis))
    everything = lax.all_gather(array, axis)
    start = jnp.broadcast_to(jnp.asarray(identity, array.dtype), array.shape)

    def lap(k, before):
        reached = k < mine
        new = combine(before, everything[k])
        return jnp.where(reached, new, before)

    return lax.fori_loop(0, length, lap, start)


def in_order(blocks, dim):
    blocks = jnp.moveaxis(blocks, 0, dim)
    lengths = blocks.shape
    return blocks.reshape(*lengths[:dim], lengths[dim] * lengths[dim + 1], *lengths[dim + 2 :])


def stacked_from(array, axes, turns):
    blocks = array
    for k in turns:
        blocks = lax.all_gather(blocks, axes[k])
    done = turns[::-1]
    back = [done.index(k) for k in range(len(axes))]
    blocks = blocks.transpose(*back, *range(len(axes), blocks.ndim))
    return blocks.reshape(-1, *array.shape)


def whole_of(array, axes, turns, dim):
    return in_order(stacked_from(array, axes, turns), dim)


def sent_to_all(array, axis):
    length = lax.axis_size(axis)
    return lax.all_to_all(
        jnp.broadcast_to(array[None], (length, *array.shape)), axis, 0, 0, tiled=True
    )


def gathered_copies(array, axis, dim):
    blocks = sent_to_all(array, axis)
    return in_order(blocks, dim)


def norm_rows(rows, gain):
    wide = rows.astype(jnp.float32)
    scale = lax.rsqrt(jnp.mean(wide * wide, axis=-1, keepdims=True) + 1e-06)
    return (wide * scale * gain).astype(jnp.bfloat16)


def add_terms(earlier, later):
    return earlier + later


def merge_state(state, part):
    peak, total, numer = state
    new_peak, new_total, new_numer = part
    highest = jnp.maximum(peak, new_peak)
    keep = jnp.exp(peak - highest)
    fresh = jnp.exp(new_peak - highest)
    return (
        highest,
        total * keep + new_total * fresh,
        numer * keep[..., None] + new_numer * fresh[..., None],
    )


def group_partial(query, query_index, group_kv, group_bias, group, past_rows, new_rows):
    head_width = query.shape[-1]
    keys = group_kv[..., :head_width]
    values = group_kv[..., head_width:]
    score = jnp.einsum("bkgd,nkd->bkgn", query, keys, preferred_element_type=jnp.float32)
    score = score * head_width ** (-0.5) + group_bias[None]
    rank = jnp.arange(group_kv.shape[0], dtype=jnp.int32)
    new_index = group * new_rows + rank - past_rows
    visible = (rank < past_rows)[None, :] | (new_index[None, :] <= query_index[:, None])
    score = jnp.where(visible[:, None, None, :], score, -jnp.inf)
    peak = jnp.max(score, axis=-1)
    weight = jnp.exp(score - peak[..., None])
    total = jnp.sum(weight, axis=-1)
    numer = jnp.einsum(
        "bkgn,nkd->bkgd", weight.astype(jnp.bfloat16), values, preferred_element_type=jnp.float32
    )
    return (peak, total, numer)


def decode_attention(query, new_key, new_value, new_gate, cache, gate, lengths):
    seqs, pairs_here, group_size, head_width = query.shape
    span = cache.shape[1]
    keys = cache[..., :head_width]
    values = cache[..., head_width:]
    target_location = jnp.arange(span, dtype=jnp.int32)
    last_gate = jnp.sum(
        jnp.where(target_location[None, None, :] == lengths[:, None, None] - 1, gate, 0.0), axis=-1
    )
    score = jnp.einsum(
        "skgd,slkd->skgl", query, keys, preferred_element_type=jnp.float32
    ) * head_width ** (-0.5)
    score = score - gate.reshape(seqs, pairs_here, group_size, span)
    score = jnp.where(
        (target_location[None, :] < lengths[:, None])[:, None, None, :], score, -jnp.inf
    )
    own = jnp.einsum(
        "skgd,skd->skg", query, new_key, preferred_element_type=jnp.float32
    ) * head_width ** (-0.5)
    own = own - (last_gate + new_gate).reshape(seqs, pairs_here, group_size)
    peak = jnp.maximum(jnp.max(score, axis=-1), own)
    weight = jnp.exp(score - peak[..., None])
    own_weight = jnp.exp(own - peak)
    total = jnp.sum(weight, axis=-1) + own_weight
    numer = jnp.einsum(
        "skgl,slkd->skgd", weight.astype(jnp.bfloat16), values, preferred_element_type=jnp.float32
    )
    numer = numer + own_weight.astype(jnp.bfloat16).astype(jnp.float32)[..., None] * new_value[
        :, :, None, :
    ].astype(jnp.float32)
    return numer / total[..., None]


def local(
    piece_rows,
    dec_rows,
    norm_gain,
    w_query,
    w_key,
    w_value,
    w_forget,
    forget_bias,
    piece_decay,
    cache_kv,
    cache_gate,
    dec_cache,
    dec_gate,
    dec_lengths,
    w_out,
):
    piece_count = piece_rows.shape[0]
    dec_count = dec_rows.shape[0]
    past_rows = cache_kv.shape[0]
    pairs_here = cache_kv.shape[1]
    head_width = cache_kv.shape[2] // 2
    heads_here = w_forget.shape[1]
    group_size = heads_here // pairs_here
    group_rows = past_rows + piece_count
    normed = norm_rows(jnp.concatenate([piece_rows, dec_rows], axis=0), norm_gain)
    query = jnp.dot(normed, w_query, preferred_element_type=jnp.float32).astype(jnp.bfloat16)
    new_key = jnp.dot(normed, w_key, preferred_element_type=jnp.float32).astype(jnp.bfloat16)
    new_value = jnp.dot(normed, w_value, preferred_element_type=jnp.float32).astype(jnp.bfloat16)
    log_gate = jax.nn.log_sigmoid(
        jnp.dot(normed, w_forget, preferred_element_type=jnp.float32) + forget_bias
    )
    piece_gate = log_gate[:piece_count] + piece_decay.T
    running = jnp.cumsum(piece_gate, axis=0)
    before = carried_in(running[-1], KV, add_terms, jnp.zeros((heads_here,), jnp.float32))
    new_bias = -(running + before[None, :]).T
    piece_kv = jnp.concatenate(
        [
            new_key[:piece_count].reshape(piece_count, pairs_here, head_width),
            new_value[:piece_count].reshape(piece_count, pairs_here, head_width),
        ],
        axis=-1,
    )
    group_kv = jnp.concatenate([cache_kv, piece_kv], axis=0)
    group_bias = jnp.concatenate([cache_gate, new_bias], axis=1)
    my_group = lax.axis_index(KV)
    every_bias = whole_of(group_bias, KV, (0, 1), 1)
    own_query = query[:piece_count].reshape(piece_count, pairs_here, group_size, head_width)
    own_index = my_group * piece_count + jnp.arange(piece_count, dtype=jnp.int32)
    start_state = (
        jnp.full((piece_count, pairs_here, group_size), -jnp.inf, jnp.float32),
        jnp.zeros((piece_count, pairs_here, group_size), jnp.float32),
        jnp.zeros((piece_count, pairs_here, group_size, head_width), jnp.float32),
    )
    state = start_state
    piece = lax.all_gather(group_kv, KV, axis=0, tiled=True)
    count = piece.shape[0] // group_rows
    blocks = piece.reshape(count, group_rows, pairs_here, 2 * head_width)

    def visit(carry, item):
        block, offset = item
        bias = lax.dynamic_slice_in_dim(every_bias, offset * group_rows, group_rows, 1)
        part = group_partial(
            own_query,
            own_index,
            block,
            bias.reshape(pairs_here, group_size, group_rows),
            offset,
            past_rows,
            piece_count,
        )
        return (merge_state(carry, part), None)

    state, _ = lax.scan(visit, state, (blocks, jnp.arange(count, dtype=jnp.int32)))
    peak, total, numer = state
    piece_attn = numer / total[..., None]
    dec_attn = decode_attention(
        query[piece_count:].reshape(dec_count, pairs_here, group_size, head_width),
        new_key[piece_count:].reshape(dec_count, pairs_here, head_width),
        new_value[piece_count:].reshape(dec_count, pairs_here, head_width),
        log_gate[piece_count:],
        dec_cache,
        dec_gate,
        dec_lengths,
    )
    attn_rows = jnp.concatenate(
        [
            piece_attn.reshape(piece_count, heads_here * head_width),
            dec_attn.reshape(dec_count, heads_here * head_width),
        ],
        axis=0,
    ).astype(jnp.bfloat16)
    every_head = gathered_copies(attn_rows, "tp", 1)
    mixed = jnp.dot(every_head, w_out, preferred_element_type=jnp.float32).astype(jnp.bfloat16)
    return (mixed[:piece_count], mixed[piece_count:])


def solution(mesh):
    finer = Mesh(
        mesh.devices.reshape(mesh.shape["grp"], 32, 2, mesh.shape["tp"]),
        ("grp", "kv_0", "kv_1", "tp"),
    )
    return jax.shard_map(
        local,
        mesh=finer,
        in_specs=(
            P(GRP_KV, None),
            P(GRP_KV, None),
            P(),
            P(None, "tp"),
            P(None, "tp"),
            P(None, "tp"),
            P(None, "tp"),
            P("tp"),
            P("tp", GRP_KV),
            P(GRP_KV, "tp", None),
            P("tp", GRP_KV),
            P(GRP_KV, None, "tp", None),
            P(GRP_KV, "tp", None),
            P(GRP_KV),
            P(None, "tp"),
        ),
        out_specs=(P(GRP_KV, "tp"), P(GRP_KV, "tp")),
        check_vma=False,
    )
```

profile of v0, /device:TPU:33, one launch (start us, length us, event | category | flops | bytes accessed | tf_op | source)
XLA Modules:
  0.0 496.2 jit_solution(10533658309555598775)
XLA Ops:
  7.3 1.2 fusion.35
  8.6 1.4 convolution_convert_fusion.2
  10.0 1.4 convolution_convert_fusion.3
  12.3 1.7 convolution_convert_fusion.1
  14.9 96.8 %all-gather.2 = f32[64,1,4]{2,1,0:T(1,128)S(1)} all-gather(f32[1,1,4]{2,1,0:T(1,128)S(1)} %slice_bitcast_fusion.7), channel_id=1, replica_groups=mesh['grp'=2,'kv_0'=32,'kv_1'=2,'tp'=4] {'kv_0','kv_1'}, dimensions={0}, use_global_device_ids=true | all-gather | bytes 1040 | tf_op jit(solution)/shard_map/all_gather | solution.py:13
  111.8 2.6 while.31
  117.1 46.0 %all-gather.3 = f32[32,4,832]{2,1,0:T(4,128)S(1)} all-gather(f32[1,4,832]{2,1,0:T(4,128)S(1)} %maximum_bitcast_fusion), channel_id=2, replica_groups=mesh['grp'=2,'kv_0'=32,'kv_1'=2,'tp'=4] {'kv_0'}, dimensions={0}, use_global_device_ids=true | all-gather | bytes 439296 | tf_op jit(solution)/shard_map/all_gather | solution.py:33
  163.1 11.7 %all-gather.1 = f32[64,4,832]{2,1,0:T(4,128)S(1)} all-gather(f32[32,4,832]{2,1,0:T(4,128)S(1)} %all-gather.3), channel_id=3, replica_groups=mesh['grp'=2,'kv_0'=32,'kv_1'=2,'tp'=4] {'kv_1'}, dimensions={0}, use_global_device_ids=true | all-gather | bytes 1277952 | tf_op jit(solution)/shard_map/all_gather | solution.py:33
  175.6 12.4 %all-gather.6.cloned.1.call-done = bf16[53248,1,128]{2,0,1:T(8,128)(2,1)} async-done(((bf16[832,1,128]{2,0,1:T(8,128)(2,1)}), bf16[53248,1,128]{2,0,1:T(8,128)(2,1)}) %all-gather.6.cloned.1.call-update) | async-done | bytes 13631504 | tf_op jit(solution)/shard_map/all_gather | solution.py:186
  188.0 290.5 %while.32 = (s32[]{:T(128)}, f32[64,1,4]{0,2,1:T(4,128)S(1)}, f32[64,1,4]{0,2,1:T(4,128)S(1)}, f32[64,1,4,64]{0,3,2,1:T(8,128)S(1)}, s32[64]{0:T(128)S(1)}, /*in...) while((s32[]{:T(128)}, f32[64,1,4]{0,2,1:T(4,128)S(1)}, ...), condition=%wide.region_7.8_spmd.clone, body=%wide.region_4.7_spmd.clone.sunk | while | flops 56406536 | bytes 4148079 | solution.py:204
  190.1 1.0 constant_dynamic-slice_fusion.5
  194.7 1.0 constant_dynamic-slice_fusion.5
  199.2 1.0 constant_dynamic-slice_fusion.5
  203.7 1.0 constant_dynamic-slice_fusion.5
  208.3 1.0 constant_dynamic-slice_fusion.5
  212.8 1.0 constant_dynamic-slice_fusion.5
  217.4 1.0 constant_dynamic-slice_fusion.5
  221.9 1.0 constant_dynamic-slice_fusion.5
  226.4 1.0 constant_dynamic-slice_fusion.5
  231.0 1.0 constant_dynamic-slice_fusion.5
  235.5 1.0 constant_dynamic-slice_fusion.5
  240.1 1.0 constant_dynamic-slice_fusion.5
  244.6 1.0 constant_dynamic-slice_fusion.5
  249.1 1.0 constant_dynamic-slice_fusion.5
  253.7 1.0 constant_dynamic-slice_fusion.5
  258.2 1.0 constant_dynamic-slice_fusion.5
  262.8 1.0 constant_dynamic-slice_fusion.5
  267.3 1.0 constant_dynamic-slice_fusion.5
  271.8 1.0 constant_dynamic-slice_fusion.5
  276.4 1.0 constant_dynamic-slice_fusion.5
  280.9 1.0 constant_dynamic-slice_fusion.5
  285.4 1.0 constant_dynamic-slice_fusion.5
  290.0 1.0 constant_dynamic-slice_fusion.5
  294.5 1.0 constant_dynamic-slice_fusion.5
  299.1 1.0 constant_dynamic-slice_fusion.5
  303.6 1.0 constant_dynamic-slice_fusion.5
  308.1 1.0 constant_dynamic-slice_fusion.5
  312.7 1.0 constant_dynamic-slice_fusion.5
  317.2 1.0 constant_dynamic-slice_fusion.5
  321.8 1.0 constant_dynamic-slice_fusion.5
  326.3 1.0 constant_dynamic-slice_fusion.5
  330.8 1.0 constant_dynamic-slice_fusion.5
  335.4 1.0 constant_dynamic-slice_fusion.5
  339.9 1.0 constant_dynamic-slice_fusion.5
  344.5 1.0 constant_dynamic-slice_fusion.5
  349.0 1.0 constant_dynamic-slice_fusion.5
  353.5 1.0 constant_dynamic-slice_fusion.5
  358.1 1.0 constant_dynamic-slice_fusion.5
  362.6 1.0 constant_dynamic-slice_fusion.5
  367.1 1.0 constant_dynamic-slice_fusion.5
  371.7 1.0 constant_dynamic-slice_fusion.5
  376.2 1.0 constant_dynamic-slice_fusion.5
  380.8 1.0 constant_dynamic-slice_fusion.5
  385.3 1.0 constant_dynamic-slice_fusion.5
  389.8 1.0 constant_dynamic-slice_fusion.5
  394.4 1.0 constant_dynamic-slice_fusion.5
  398.9 1.0 constant_dynamic-slice_fusion.5
  403.5 1.0 constant_dynamic-slice_fusion.5
  408.0 1.0 constant_dynamic-slice_fusion.5
  412.5 1.0 constant_dynamic-slice_fusion.5
  439.8 1.0 constant_dynamic-slice_fusion.5
  453.4 1.0 constant_dynamic-slice_fusion.5
  476.1 1.0 constant_dynamic-slice_fusion.5
  478.6 9.1 %all_to_all.5 = bf16[4,66,256]{2,1,0:T(8,128)(2,1)S(1)} all-to-all(bf16[4,66,256]{2,1,0:T(8,128)(2,1)S(1)} %broadcast_in_dim.84), channel_id=1, replica_groups=mesh['grp'=2,'kv_0'=32,'kv_1'=2,'tp'=4] {'tp'}, dimensions={0} | all-to-all | bytes 270336 | tf_op jit(solution)/shard_map/all_to_all | solution.py:46
  (987 shorter events, 159.4 us)
Async XLA Ops:
  7.2 480.7 %copy-start = (bf16[1024,512]{1,0:T(8,128)(2,1)S(1)}, bf16[1024,512]{1,0:T(8,128)(2,1)}, u32[]{:S(2)}) copy-start(bf16[1024,512]{1,0:T(8,128)(2,1)} %param.33) | copy-start | bytes 3145732
  7.2 5.1 %copy-start.6 = (bf16[2,2048]{1,0:T(2,128)(2,1)S(1)}, bf16[2,2048]{1,0:T(2,128)(2,1)}, u32[]{:S(2)}) copy-start(bf16[2,2048]{1,0:T(2,128)(2,1)} %param.20) | copy-start | bytes 24580
  7.2 5.1 %copy-start.3 = (bf16[64,2048]{1,0:T(8,128)(2,1)S(1)}, bf16[64,2048]{1,0:T(8,128)(2,1)}, u32[]{:S(2)}) copy-start(bf16[64,2048]{1,0:T(8,128)(2,1)} %param.19) | copy-start | bytes 786436
  7.2 5.1 %copy-start.10 = (f32[2048]{0:T(1024)S(1)}, f32[2048]{0:T(1024)}, u32[]{:S(2)}) copy-start(f32[2048]{0:T(1024)} %param.21) | copy-start | bytes 24580
  7.2 4.2 copy-start.4
  7.2 180.8 %all-gather.6.cloned.1.call-start = ((), (), s32[]{:S(2)}) async-start(), calls=%async_computation.1 | async-start | bytes 13844480 | tf_op jit(solution)/shard_map/all_gather | solution.py:186
  9.9 4.1 copy-start.8
  9.9 4.2 copy-start.2
  10.0 4.4 copy-start.9
  10.0 4.4 copy-start.11
  11.4 3.3 copy-start.7
  12.3 102.6 %copy-start.1 = (bf16[2,3072,1,128]{3,1,2,0:T(8,128)(2,1)S(1)}, bf16[2,3072,1,128]{3,1,2,0:T(8,128)(2,1)}, u32[]{:S(2)}) copy-start(bf16[2,3072,1,128]{3,1,2,0:T(8,128)(2,1)} %param.30) | copy-start | bytes 4718596
  115.0 2.1 copy-start.5
Sparse Core Ops, SparseCore 0:
  12.4 175.5 all-gather.5
where the time goes:
time: 499 us; the launch traced here: 496 us
  blocking collectives  164 us (33%)
  local copies, waits for them, and re-layouts  118 us (24%)
  loops' own time  90.1 us (18%)
  matrix products  64.2 us (13%)
  other arithmetic  33.3 us (7%)
  between operations  14.5 us (3%)
  waiting for transfers between devices  12.5 us (3%)
    dynamic_slice x192, local copies, waits for them, and re-layouts, local(): lax.scan(visit, state, (blocks, jnp.arange(count, dtype=jnp.int32)))  109 us
    all_gather x1, blocking collectives, carried_in(): everything = lax.all_gather(array, axis)  96.8 us
    another operation x1, loops' own time, local(): lax.scan(visit, state, (blocks, jnp.arange(count, dtype=jnp.int32)))  88.6 us
    all_gather x2, blocking collectives, stacked_from(): blocks = lax.all_gather(blocks, axes[k])  57.7 us
    dot_general x64, matrix products, group_partial(): jnp.einsum('bkgn,nkd->bkgd', weight.astype(jnp.bfloat16), values, preferr...  33.8 us
    dot_general x64, matrix products, group_partial(): jnp.einsum('bkgd,nkd->bkgn', query, keys, preferred_element_type=jnp.floa...  24 us
    reduce_sum x64, other arithmetic, group_partial(): total = jnp.sum(weight, axis=-1)  19.4 us
    all_gather x1, waiting for transfers between devices, local(): piece = lax.all_gather(group_kv, KV, axis=0, tiled=True)  12.4 us
  transfers between devices with their start and end apart: 1, of which 1 were waited for; matrix products, arithmetic and copies ran while one was open for 1% of the time, Pallas kernels for 0%

commit v1 on v0

--- a/solution.py
+++ b/solution.py
@@ -183,7 +183,9 @@
         jnp.zeros((piece_count, pairs_here, group_size, head_width), jnp.float32),
     )
     state = start_state
-    piece = lax.all_gather(group_kv, KV, axis=0, tiled=True)
+    piece = jnp.concatenate(
+        lax.all_to_all(jnp.stack([group_kv] * lax.axis_size(KV)), KV, 0, 0), axis=0
+    )
     count = piece.shape[0] // group_rows
     blocks = piece.reshape(count, group_rows, pairs_here, 2 * head_width)
 

time: 499 us -> 1660 us (3.33)
  blocking collectives: 164 us -> 1280 us
  starting transfers between devices: 0.06 us -> 47.6 us
    all_gather x1, blocking collectives: 96.8 us -> 1220 us  [carried_in(): everything = lax.all_gather(array, axis)]
    all_to_all x0 -> x1, starting transfers between devices: none -> 47.6 us  [local(): lax.all_to_all(jnp.stack([group_kv] * lax.axis_size(KV)), KV, 0, 0)]
  transfers between devices with their start and end apart: 1 -> 1, of which waited for: 1 -> 0; matrix products, arithmetic and copies ran while one was open for 1% -> 0% of each run, Pallas kernels for 0% -> 0%
where the time goes in v1:
time: 1660 us; the launch traced here: 1650 us
  blocking collectives  1280 us (77%)
  local copies, waits for them, and re-layouts  130 us (8%)
  loops' own time  94.1 us (6%)
  matrix products  64.4 us (4%)
  starting transfers between devices  47.6 us (3%)
  other arithmetic  31.9 us (2%)
    all_gather x1, blocking collectives, carried_in(): everything = lax.all_gather(array, axis)  1220 us
    dynamic_slice x192, local copies, waits for them, and re-layouts, local(): lax.scan(visit, state, (blocks, jnp.arange(count, dtype=jnp.int32)))  113 us
    another operation x1, loops' own time, local(): lax.scan(visit, state, (blocks, jnp.arange(count, dtype=jnp.int32)))  92.6 us
    all_gather x2, blocking collectives, stacked_from(): blocks = lax.all_gather(blocks, axes[k])  56.6 us
    all_to_all x1, starting transfers between devices, local(): lax.all_to_all(jnp.stack([group_kv] * lax.axis_size(KV)), KV, 0, 0)  47.6 us
    dot_general x64, matrix products, group_partial(): jnp.einsum('bkgn,nkd->bkgd', weight.astype(jnp.bfloat16), values, preferr...  33.9 us
  transfers between devices with their start and end apart: 1, of which 0 were waited for; matrix products, arithmetic and copies ran while one was open for 0% of the time, Pallas kernels for 0%

profile of v1, /device:TPU:33, one launch (start us, length us, event | category | flops | bytes accessed | tf_op | source)
XLA Modules:
  0.0 1652.7 jit_solution(13143176417820395110)
XLA Ops:
  0.7 1.2 fusion.35
  1.9 1.4 convolution_convert_fusion.3
  3.3 1.4 convolution_convert_fusion.2
  4.8 8.2 stack.2
  13.0 47.6 %all-to-all-start = ((bf16[64,832,1,128]{3,1,2,0:T(8,128)(2,1)}), bf16[64,832,1,128]{3,1,2,0:T(8,128)(2,1)}, u32[]{:S(2)}, u32[]{:S(2)}) async-start(bf16[64,832,1,128]{3,1,2,0:T(8,128)(2,1)} %stack.2), calls=%async_computation | async-start | bytes 27262976 | tf_op jit(solution)/shard_map/all_to_all | solution.py:187
  60.7 1.7 convolution_convert_fusion.1
  65.7 1216.4 %all-gather.2 = f32[64,1,4]{2,1,0:T(1,128)S(1)} all-gather(f32[1,1,4]{2,1,0:T(1,128)S(1)} %slice_bitcast_fusion.7), channel_id=1, replica_groups=mesh['grp'=2,'kv_0'=32,'kv_1'=2,'tp'=4] {'kv_0','kv_1'}, dimensions={0}, use_global_device_ids=true | all-gather | bytes 1040 | tf_op jit(solution)/shard_map/all_gather | solution.py:13
  1282.1 2.6 while.31
  1284.8 40.9 %all-gather.3 = f32[32,4,832]{2,1,0:T(4,128)S(1)} all-gather(f32[1,4,832]{2,1,0:T(4,128)S(1)} %maximum_bitcast_fusion.1), channel_id=2, replica_groups=mesh['grp'=2,'kv_0'=32,'kv_1'=2,'tp'=4] {'kv_0'}, dimensions={0}, use_global_device_ids=true | all-gather | bytes 439296 | tf_op jit(solution)/shard_map/all_gather | solution.py:33
  1325.7 15.7 all-gather.1
  1342.4 297.9 %while.32 = (s32[]{:T(128)}, f32[64,1,4]{0,2,1:T(4,128)S(1)}, f32[64,1,4]{0,2,1:T(4,128)S(1)}, f32[64,1,4,64]{0,3,2,1:T(8,128)S(1)}, s32[64]{0:T(128)S(1)}, /*in...) while((s32[]{:T(128)}, f32[64,1,4]{0,2,1:T(4,128)S(1)}, ...), condition=%wide.region_7.8_spmd.clone, body=%wide.region_4.7_spmd.clone.sunk | while | flops 56406536 | bytes 4148071 | solution.py:206
  1344.6 1.0 constant_dynamic-slice_fusion.5
  1349.3 1.0 constant_dynamic-slice_fusion.5
  1353.9 1.0 constant_dynamic-slice_fusion.5
  1358.6 1.0 constant_dynamic-slice_fusion.5
  1363.2 1.0 constant_dynamic-slice_fusion.5
  1367.9 1.0 constant_dynamic-slice_fusion.5
  1372.5 1.0 constant_dynamic-slice_fusion.5
  1377.2 1.0 constant_dynamic-slice_fusion.5
  1381.9 1.0 constant_dynamic-slice_fusion.5
  1386.5 1.0 constant_dynamic-slice_fusion.5
  1391.2 1.0 constant_dynamic-slice_fusion.5
  1395.8 1.0 constant_dynamic-slice_fusion.5
  1400.5 1.0 constant_dynamic-slice_fusion.5
  1405.1 1.0 constant_dynamic-slice_fusion.5
  1409.8 1.0 constant_dynamic-slice_fusion.5
  1414.4 1.0 constant_dynamic-slice_fusion.5
  1419.1 1.0 constant_dynamic-slice_fusion.5
  1423.7 1.0 constant_dynamic-slice_fusion.5
  1428.4 1.0 constant_dynamic-slice_fusion.5
  1433.1 1.0 constant_dynamic-slice_fusion.5
  1437.7 1.0 constant_dynamic-slice_fusion.5
  1442.4 1.0 constant_dynamic-slice_fusion.5
  1447.0 1.0 constant_dynamic-slice_fusion.5
  1451.7 1.0 constant_dynamic-slice_fusion.5
  1456.3 1.0 constant_dynamic-slice_fusion.5
  1461.0 1.0 constant_dynamic-slice_fusion.5
  1465.6 1.0 constant_dynamic-slice_fusion.5
  1470.3 1.0 constant_dynamic-slice_fusion.5
  1475.0 1.0 constant_dynamic-slice_fusion.5
  1479.6 1.0 constant_dynamic-slice_fusion.5
  1484.3 1.0 constant_dynamic-slice_fusion.5
  1488.9 1.0 constant_dynamic-slice_fusion.5
  1493.6 1.0 constant_dynamic-slice_fusion.5
  1498.2 1.0 constant_dynamic-slice_fusion.5
  1502.9 1.0 constant_dynamic-slice_fusion.5
  1507.5 1.0 constant_dynamic-slice_fusion.5
  1512.2 1.0 constant_dynamic-slice_fusion.5
  1516.8 1.0 constant_dynamic-slice_fusion.5
  1521.5 1.0 constant_dynamic-slice_fusion.5
  1526.2 1.0 constant_dynamic-slice_fusion.5
  1530.8 1.0 constant_dynamic-slice_fusion.5
  1535.5 1.0 constant_dynamic-slice_fusion.5
  1540.1 1.0 constant_dynamic-slice_fusion.5
  1544.8 1.0 constant_dynamic-slice_fusion.5
  1549.4 1.0 constant_dynamic-slice_fusion.5
  1554.1 1.0 constant_dynamic-slice_fusion.5
  1558.7 1.0 constant_dynamic-slice_fusion.5
  1563.4 1.0 constant_dynamic-slice_fusion.5
  1568.0 1.0 constant_dynamic-slice_fusion.5
  1582.0 1.0 constant_dynamic-slice_fusion.5
  1586.7 1.0 constant_dynamic-slice_fusion.5
  1596.0 1.0 constant_dynamic-slice_fusion.5
  1640.4 10.6 all_to_all.10
  (990 shorter events, 163.0 us)
Async XLA Ops:
  0.6 1650.5 %copy-start = (bf16[1024,512]{1,0:T(8,128)(2,1)S(1)}, bf16[1024,512]{1,0:T(8,128)(2,1)}, u32[]{:S(2)}) copy-start(bf16[1024,512]{1,0:T(8,128)(2,1)} %param.33) | copy-start | bytes 3145732
  0.6 4.0 copy-start.4
  12.9 47.7 %copy-start.3 = (bf16[64,2048]{1,0:T(8,128)(2,1)S(1)}, bf16[64,2048]{1,0:T(8,128)(2,1)}, u32[]{:S(2)}) copy-start(bf16[64,2048]{1,0:T(8,128)(2,1)} %param.19) | copy-start | bytes 786436
  12.9 47.7 %copy-start.7 = (bf16[2,2048]{1,0:T(2,128)(2,1)S(1)}, bf16[2,2048]{1,0:T(2,128)(2,1)}, u32[]{:S(2)}) copy-start(bf16[2,2048]{1,0:T(2,128)(2,1)} %param.20) | copy-start | bytes 24580
  13.0 47.7 %copy-start.11 = (f32[2048]{0:T(1024)S(1)}, f32[2048]{0:T(1024)}, u32[]{:S(2)}) copy-start(f32[2048]{0:T(1024)} %param.21) | copy-start | bytes 24580
  13.0 49.8 %copy-start.2 = (f32[2,4,3072]{2,1,0:T(4,128)S(1)}, f32[2,4,3072]{2,1,0:T(4,128)}, u32[]{:S(2)}) copy-start(f32[2,4,3072]{2,1,0:T(4,128)} %param.31) | copy-start | bytes 294916
  13.0 1329.4 %all-to-all-start = ((bf16[64,832,1,128]{3,1,2,0:T(8,128)(2,1)}), bf16[64,832,1,128]{3,1,2,0:T(8,128)(2,1)}, u32[]{:S(2)}, u32[]{:S(2)}) async-start(bf16[64,832,1,128]{3,1,2,0:T(8,128)(2,1)} %stack.2), calls=%async_computation | async-start | bytes 27262976 | tf_op jit(solution)/shard_map/all_to_all | solution.py:187
  60.6 2.1 copy-start.9
  60.6 2.2 copy-start.1
  60.6 3.2 copy-start.10
  60.6 3.2 copy-start.12
  62.3 3.1 copy-start.5
  63.4 2.1 copy-start.8
  63.7 1221.0 %copy-start.6 = (f32[4,768]{1,0:T(4,128)S(1)}, f32[4,768]{1,0:T(4,128)}, u32[]{:S(2)}) copy-start(f32[4,768]{1,0:T(4,128)} %param.29) | copy-start | bytes 36868
  1341.5 0.8 slice-start
